TPU v7x, 128 devices: a whole 4x4x4 slice. The times are simulated.
128 devices in a mesh: sp: 16 (over z, x), tp: 8 (over y, core).
Axes of the slice: x: 4, y: 4, z: 4, core: 2. Of those that a mesh axis runs over, the one named last changes fastest.
Arguments:
- queries: bfloat16 [16384, 1024], P('sp', 'tp'), may hold values from -75 to 75
- key_rows: bfloat16 [16384, 1024], P('sp', 'tp'), may hold values from -4 to 4
- value_rows: bfloat16 [16384, 1024], P('sp', 'tp'), may hold values from -6 to 6
- cum_gate: float32 [16, 16384], P('tp'), may hold values from -2342 to 0, as said below
- residual: bfloat16 [16384, 2048], P(('sp', 'tp')), may hold values from -6 to 6
- out_weight: bfloat16 [1024, 2048], replicated, may hold values from -0.1875 to 0.1875
- gain_mix: float32 [2048], replicated, may hold values from 0.1 to 1.9
- gain_pre: float32 [2048], replicated, may hold values from 0.1 to 1.9
- gain_post: float32 [2048], replicated, may hold values from 0.1 to 1.9
- route_ids: int32 [16384, 2], P(('sp', 'tp')), may hold values from 0 to 127, all different within a row; in each aligned block of 128 rows (0 to 127, 128 to 255, ...) at most 3 rows name the same one
- route_weight: float32 [16384, 2], P(('sp', 'tp')), may hold values from 0.2 to 1
- w_gate: bfloat16 [128, 2048, 512], P(('sp', 'tp')), may hold values from -0.125 to 0.125
- w_up: bfloat16 [128, 2048, 512], P(('sp', 'tp')), may hold values from -0.125 to 0.125
- w_down: bfloat16 [128, 512, 2048], P(('sp', 'tp')), may hold values from -0.25 to 0.25
Outputs:
- layer_out: bfloat16 [16384, 2048], P(('sp', 'tp'))
Inputs may be any that keep to these rules, and one draw needn't show every extreme that they name: `route_ids`: each row names 2 different experts; in the rows of one device no expert is named more than 3 times, a bound that some block reaches. `cum_gate`: along the positions each head's values never rise.
All inputs are finite; a program needn't handle non-finite values.
Results may differ from a plain program's by a relative error of at most 0.018.
Values may be sent and summed in bfloat16 or wider, within the bound.
A program may use at most 64 MiB of HBM per device.

v0:
```python
import math
import jax
import jax.numpy as jnp
from jax import lax
from jax.sharding import PartitionSpec as P

HEAD_DIM = 64
NORM_EPS = 1e-06
MASKED = -1e30


def rms_scale(rows, gain):
    mean_sq = jnp.mean(rows * rows, axis=-1, keepdims=True)
    return rows * lax.rsqrt(mean_sq + NORM_EPS) * gain


def attend(running, queries, gate_q, q_start, key_part, value_part, gate_k, k_start):
    row_peak, row_total, weighted = running
    scores = jnp.einsum(
        "qhd,khd->hqk", queries, key_part, preferred_element_type=jnp.float32
    ) * HEAD_DIM ** (-0.5)
    scores = scores + gate_q[:, :, None] - gate_k[:, None, :]
    query_pos = q_start + lax.iota(jnp.int32, queries.shape[0])
    key_pos = k_start + lax.iota(jnp.int32, key_part.shape[0])
    allowed = (key_pos[None, :] <= query_pos[:, None])[None]
    scores = jnp.where(allowed, scores, MASKED)
    new_peak = jnp.maximum(row_peak, jnp.max(scores, axis=-1))
    unnorm = jnp.where(allowed, jnp.exp(scores - new_peak[..., None]), 0.0)
    rescale = jnp.exp(row_peak - new_peak)
    row_total = row_total * rescale + jnp.sum(unnorm, axis=-1)
    weighted = weighted * rescale.T[:, :, None] + jnp.einsum(
        "hqk,khd->qhd", unnorm.astype(jnp.bfloat16), value_part, preferred_element_type=jnp.float32
    )
    return (new_peak, row_total, weighted)


def local(
    queries,
    key_rows,
    value_rows,
    cum_gate,
    residual,
    out_weight,
    gain_mix,
    gain_pre,
    gain_post,
    route_ids,
    route_weight,
    w_gate,
    w_up,
    w_down,
):
    tok_dev, feature_width = queries.shape
    local_heads = feature_width // HEAD_DIM
    my_start = lax.axis_index("sp") * tok_dev
    query_heads = queries.reshape(tok_dev, local_heads, HEAD_DIM)
    gate_q = lax.dynamic_slice_in_dim(cum_gate, my_start, tok_dev, 1)
    initial = (
        jnp.full((local_heads, tok_dev), MASKED, jnp.float32),
        jnp.zeros((local_heads, tok_dev), jnp.float32),
        jnp.zeros((tok_dev, local_heads, HEAD_DIM), jnp.float32),
    )
    paired = jnp.stack((key_rows, value_rows))

    def consume(running, key_part, value_part, k_start):
        row_count = key_part.shape[0]
        gate_k = lax.dynamic_slice_in_dim(cum_gate, k_start, row_count, 1)
        return attend(
            running,
            query_heads,
            gate_q,
            my_start,
            key_part.reshape(row_count, local_heads, HEAD_DIM),
            value_part.reshape(row_count, local_heads, HEAD_DIM),
            gate_k,
            k_start,
        )

    running = initial
    piece = lax.all_gather(paired, "sp", axis=1, tiled=True)
    row_count = piece.shape[1]
    span_rows = math.gcd(row_count, tok_dev)

    def single(block_index, running):
        offset = block_index * span_rows
        part = lax.dynamic_slice_in_dim(piece, offset, span_rows, 1)
        return lax.cond(
            offset < my_start + tok_dev,
            lambda state_now: consume(state_now, part[0], part[1], offset),
            lambda state_now: state_now,
            running,
        )

    running = lax.fori_loop(0, row_count // span_rows, single, running)
    row_peak, row_total, weighted = running
    attended = (
        (weighted / row_total.T[:, :, None]).astype(jnp.bfloat16).reshape(tok_dev, feature_width)
    )
    head_rows = lax.all_to_all(attended, "tp", split_axis=0, concat_axis=1, tiled=True)
    projected = jnp.dot(head_rows, out_weight, preferred_element_type=jnp.float32)
    stream = (residual.astype(jnp.float32) + rms_scale(projected, gain_mix)).astype(jnp.bfloat16)
    stream_wide = lax.optimization_barrier(stream).astype(jnp.float32)
    normed = rms_scale(stream_wide, gain_pre).astype(jnp.bfloat16)
    rows_dev, top_count = route_ids.shape
    model_width = normed.shape[1]
    experts_all = lax.axis_size("sp") * lax.axis_size("tp")
    capacity = max(2, (4 * rows_dev * top_count + 3 * experts_all - 1) // (3 * experts_all))
    flat_ids = route_ids.reshape(-1)
    onehot = (flat_ids[:, None] == lax.iota(jnp.int32, experts_all)[None, :]).astype(jnp.int32)
    slot_rank = jnp.sum(jnp.cumsum(onehot, axis=0) * onehot, axis=1) - 1
    slot_index = flat_ids * capacity + slot_rank
    spread = jnp.repeat(normed, top_count, axis=0)
    outgoing = (
        jnp.zeros((experts_all * capacity, model_width), jnp.bfloat16).at[slot_index].set(spread)
    )
    outgoing = outgoing.reshape(experts_all, capacity, model_width)
    arrived = lax.all_to_all(outgoing, ("sp", "tp"), split_axis=0, concat_axis=0, tiled=True)
    sources, slots, width_here = arrived.shape
    flat_rows = arrived.reshape(sources * slots, width_here)
    gate_act = jnp.dot(flat_rows, w_gate[0], preferred_element_type=jnp.float32)
    up_act = jnp.dot(flat_rows, w_up[0], preferred_element_type=jnp.float32)
    hidden = (jax.nn.silu(gate_act) * up_act).astype(jnp.bfloat16)
    expert_out = jnp.dot(hidden, w_down[0], preferred_element_type=jnp.float32).astype(jnp.bfloat16)
    returned = lax.all_to_all(
        expert_out.reshape(sources, slots, width_here),
        ("sp", "tp"),
        split_axis=0,
        concat_axis=0,
        tiled=True,
    )
    picked = returned.reshape(experts_all * capacity, model_width)[slot_index]
    picked = picked.reshape(rows_dev, top_count, model_width).astype(jnp.float32)
    combined = jnp.sum(picked * route_weight[:, :, None], axis=1)
    return (stream_wide + rms_scale(combined, gain_post)).astype(jnp.bfloat16)


def solution(mesh):
    return jax.shard_map(
        local,
        mesh=mesh,
        in_specs=(
            P("sp", "tp"),
            P("sp", "tp"),
            P("sp", "tp"),
            P("tp", None),
            P(("sp", "tp"), None),
            P(),
            P(),
            P(),
            P(),
            P(("sp", "tp"), None),
            P(("sp", "tp"), None),
            P(("sp", "tp"), None, None),
            P(("sp", "tp"), None, None),
            P(("sp", "tp"), None, None),
        ),
        out_specs=P(("sp", "tp"), None),
        check_vma=False,
    )
```

profile of v0, /device:TPU:1, one launch (start us, length us, event | category | flops | bytes accessed | tf_op | source)
XLA Modules:
  0.0 409.1 jit_solution(8245087762462546506)
XLA Ops:
  6.5 0.0 copy-start
  6.5 0.0 copy-start.5
  6.5 0.0 all-gather.2.cloned.1.call-start
  6.5 1.2 copy.42
  7.8 1.1 copy.43
  8.9 0.8 pad_maximum_fusion
  9.7 0.0 all-gather.2.cloned.1.call-update
  9.8 0.8 copy.47
  10.5 0.1 eq.29
  10.7 0.1 eq.25
  10.8 1.1 copy.44
  11.9 0.1 copy.49
  12.0 0.2 fusion.41
  12.3 0.7 constant_dynamic-slice_fusion.3
  13.0 0.2 fusion.42
  13.2 0.0 copy-done.5
  13.2 70.6 %all-gather.2.cloned.1.call-done = bf16[2,16384,128]{1,2,0:T(8,128)(2,1)} async-done(((bf16[2,1024,128]{1,2,0:T(8,128)(2,1)}), bf16[2,16384,128]{1,2,0:T(8,128)(2,1)}) %all-gather.2.cloned.1.call-update) | async-done | bytes 8388624 | tf_op jit(solution)/shard_map/all_gather | solution.py:80
  84.0 11.8 %while.18 = (s32[]{:T(128)}, f32[2,1024]{1,0:T(2,128)S(1)}, f32[2,1024]{1,0:T(2,128)S(1)}, f32[1024,2,64]{0,2,1:T(8,128)S(1)}, s32[]{:T(128)}, /*index=5*/s32[]{...) while((s32[]{:T(128)}, f32[2,1024]{1,0:T(2,128)S(1)}, ...), condition=%wide.region_5.6_spmd, body=%wide.region_0.5_spmd.sunk | while | flops 578035712 | bytes 32457040 | solution.py:94
  84.0 11.1 %conditional.2 = ((f32[2,1024]{1,0:T(2,128)S(1)}, f32[2,1024]{1,0:T(2,128)S(1)}, f32[1024,2,64]{0,2,1:T(8,128)S(1)})) conditional(s32[]{:T(128)} %convert_element_type.89, (f32[2,1024]{1,0:T(2,128)S(1)}, f32[2,1024]{1,0:T(2,128)S(1)}, f32[1024,2,64]{0,2,1:T(8,128)S(1)}) %tuple.52, (s32[]{:T(128)}, s32[]{:T(128)}, bf16[2,16384,128]{1,2,0:T(8,128)(2,1)}, ...), branch_computations={%region_1.0_spmd, %region_2.4_spmd} | conditional | flops 578035712 | bytes 32456802 | solution.py:87
  84.0 0.7 constant_dynamic-slice_fusion.1
  84.7 1.1 constant_dynamic-slice_fusion.2
  85.8 0.7 broadcast_compare_fusion
  86.4 2.4 fusion.2
  88.9 3.2 fusion.9
  92.1 3.0 fusion.1
  95.8 0.0 copy-start.1
  95.8 0.0 copy-start.2
  95.9 0.7 copy.45
  96.6 5.1 %all-to-all-start = ((bf16[8,128,128]{1,2,0:T(8,128)(2,1)}), bf16[8,128,128]{1,2,0:T(8,128)(2,1)S(1)}, u32[]{:S(2)}, u32[]{:S(2)}) async-start(bf16[8,128,128]{1,2,0:T(8,128)(2,1)} %copy.45), calls=%async_computation | async-start | bytes 524288 | tf_op jit(solution)/shard_map/all_to_all | solution.py:99
  101.8 0.0 copy-start.3
  101.8 0.1 copy.46
  101.9 0.1 mul.133
  102.0 6.2 %all-to-all-done = bf16[8,128,128]{1,2,0:T(8,128)(2,1)S(1)} async-done(((bf16[8,128,128]{1,2,0:T(8,128)(2,1)}), bf16[8,128,128]{1,2,0:T(8,128)(2,1)S(1)}, u32[]{:S(2)}, u32[]{:S(2)}) %all-to-all-start) | async-done | bytes 262176 | tf_op jit(solution)/shard_map/all_to_all | solution.py:99
  108.2 3.0 multiply_reduce_fusion.2
  111.3 0.0 copy-done.1
  111.3 0.0 copy-done.2
  111.3 0.2 add_convert_fusion
  111.5 0.2 fusion.27
  111.7 0.0 copy-done.3
  111.7 0.2 fusion.29
  111.9 1.7 broadcast_in_dim.62
  113.6 2.3 reshape.167
  115.8 4.1 %scatter_custom_fusion = bf16[384,2048]{1,0:T(8,128)(2,1)} fusion(s32[256]{0:T(256)S(1)} %bitcast.80, bf16[256,2048]{1,0:T(8,128)(2,1)} %reshape.167, bf16[]{:T(256)} %constant.98.clone.1), kind=kCustom, calls=%fused_computation.47 | custom fusion | bytes 1573376 | tf_op jit(solution)/shard_map/scatter | solution.py:114
  120.0 5.1 %reshape.150 = bf16[128,3,2048]{2,1,0:T(4,128)(2,1)} reshape(bf16[384,2048]{1,0:T(8,128)(2,1)} %scatter_custom_fusion) | data formatting | bytes 3145728 | tf_op jit(solution)/shard_map/reshape | solution.py:116
  125.1 202.5 %all_to_all.29 = bf16[128,3,2048]{2,1,0:T(4,128)(2,1)} all-to-all(bf16[128,3,2048]{2,1,0:T(4,128)(2,1)} %reshape.150), channel_id=1, replica_groups=mesh['sp'=16,'tp'=8] {'sp','tp'}, dimensions={0} | all-to-all | bytes 3145728 | tf_op jit(solution)/shard_map/all_to_all | solution.py:117
  327.6 5.0 %reshape.151 = bf16[384,2048]{1,0:T(8,128)(2,1)} reshape(bf16[128,3,2048]{2,1,0:T(4,128)(2,1)} %all_to_all.29) | data formatting | bytes 3145728 | tf_op jit(solution)/shard_map/reshape | solution.py:119
  332.7 3.9 fusion.19
  336.6 0.0 copy-done
  336.6 5.3 %convolution_convert_fusion = bf16[384,2048]{1,0:T(8,128)(2,1)} fusion(bf16[1,512,2048]{2,1,0:T(8,128)(2,1)S(1)} %copy-done, bf16[384,2048]{1,0:T(8,128)(2,1)} %reshape.151, bf16[1,2048,512]{2,1,0:T(8,128)(2,1)} %param.30, f32[384,512]{1,0:T(8,128)} %fusion.19), kind=kOutput, calls=%fused_computation.23 | convolution fusion | flops 1612578816 | bytes 8126464 | tf_op jit(solution)/shard_map/dot_general | solution.py:123
  341.9 0.0 copy-start.6
  341.9 5.2 %reshape.152 = bf16[128,3,2048]{2,1,0:T(4,128)(2,1)} reshape(bf16[384,2048]{1,0:T(8,128)(2,1)} %convolution_convert_fusion) | data formatting | bytes 3145728 | tf_op jit(solution)/shard_map/reshape | solution.py:125
  347.1 5.8 %all-to-all-start.2 = ((bf16[128,3,2048]{2,1,0:T(4,128)(2,1)}), bf16[128,3,2048]{2,1,0:T(4,128)(2,1)}, u32[]{:S(2)}, u32[]{:S(2)}) async-start(bf16[128,3,2048]{2,1,0:T(4,128)(2,1)} %reshape.152), calls=%async_computation.2 | async-start | bytes 4194304 | tf_op jit(solution)/shard_map/all_to_all | solution.py:124
  352.9 0.0 copy-done.6
  352.9 0.1 copy.51
  353.0 29.7 %all-to-all-done.2 = bf16[128,3,2048]{2,1,0:T(4,128)(2,1)} async-done(((bf16[128,3,2048]{2,1,0:T(4,128)(2,1)}), bf16[128,3,2048]{2,1,0:T(4,128)(2,1)}, u32[]{:S(2)}, u32[]{:S(2)}) %all-to-all-start.2) | async-done | bytes 1572896 | tf_op jit(solution)/shard_map/all_to_all | solution.py:124
  382.8 5.1 %reshape.153 = bf16[384,2048]{1,0:T(8,128)(2,1)} reshape(bf16[128,3,2048]{2,1,0:T(4,128)(2,1)} %all-to-all-done.2) | data formatting | bytes 3145728 | tf_op jit(solution)/shard_map/reshape | solution.py:131
  387.9 4.9 %gather_fusion = bf16[256,2048]{1,0:T(8,128)(2,1)} fusion(bf16[384,2048]{1,0:T(8,128)(2,1)} %reshape.153, s32[1024]{0:T(1024)S(1)} %pad_clamp_fusion), kind=kCustom, calls=%fused_computation | custom fusion | bytes 2098176 | tf_op jit(solution)/shard_map/gather | solution.py:131
  392.8 0.0 copy-start.4
  392.8 3.4 reshape.154
  396.2 4.8 %multiply_reduce_fusion = f32[128,2048]{1,0:T(8,128)S(1)} fusion(f32[128,2,2048]{2,1,0:T(2,128)} %reshape.154, f32[128,2]{1,0:T(8,128)S(1)} %copy.51), kind=kLoop, calls=%fused_computation.29 | loop fusion | flops 786432 | bytes 3146752 | tf_op jit(solution)/shard_map/reduce_sum | solution.py:133
  401.0 0.2 multiply_reduce_fusion.1
  401.2 0.0 copy-done.4
  401.2 1.0 fusion.30
  (37 shorter events, 0.5 us)
Async XLA Ops:
  6.5 330.1 %copy-start = (bf16[1,512,2048]{2,1,0:T(8,128)(2,1)S(1)}, bf16[1,512,2048]{2,1,0:T(8,128)(2,1)}, u32[]{:S(2)}) copy-start(bf16[1,512,2048]{2,1,0:T(8,128)(2,1)} %param.31) | copy-start | bytes 6291460
  6.5 6.7 %copy-start.5 = (s32[128,2]{0,1:T(2,128)S(1)}, s32[128,2]{0,1:T(2,128)}, u32[]{:S(2)}) copy-start(s32[128,2]{0,1:T(2,128)} %param.27) | copy-start | bytes 3076
  6.5 77.3 %all-gather.2.cloned.1.call-start = ((), (), s32[]{:S(2)}) async-start(), calls=%async_computation.3 | async-start | bytes 8912896 | tf_op jit(solution)/shard_map/all_gather | solution.py:80
  95.8 15.5 %copy-start.1 = (bf16[128,2048]{1,0:T(8,128)(2,1)S(1)}, bf16[128,2048]{1,0:T(8,128)(2,1)}, u32[]{:S(2)}) copy-start(bf16[128,2048]{1,0:T(8,128)(2,1)} %param.22) | copy-start | bytes 1572868
  95.8 15.5 %copy-start.2 = (f32[2048]{0:T(1024)S(1)}, f32[2048]{0:T(1024)}, u32[]{:S(2)}) copy-start(f32[2048]{0:T(1024)} %param.24) | copy-start | bytes 24580
  96.6 11.6 %all-to-all-start = ((bf16[8,128,128]{1,2,0:T(8,128)(2,1)}), bf16[8,128,128]{1,2,0:T(8,128)(2,1)S(1)}, u32[]{:S(2)}, u32[]{:S(2)}) async-start(bf16[8,128,128]{1,2,0:T(8,128)(2,1)} %copy.45), calls=%async_computation | async-start | bytes 524288 | tf_op jit(solution)/shard_map/all_to_all | solution.py:99
  101.8 10.0 %copy-start.3 = (f32[2048]{0:T(1024)S(1)}, f32[2048]{0:T(1024)}, u32[]{:S(2)}) copy-start(f32[2048]{0:T(1024)} %param.25) | copy-start | bytes 24580
  341.9 11.0 %copy-start.6 = (f32[128,2]{0,1:T(2,128)S(1)}, f32[128,2]{0,1:T(2,128)}, u32[]{:S(2)}) copy-start(f32[128,2]{0,1:T(2,128)} %param.28) | copy-start | bytes 3076
  347.1 35.7 %all-to-all-start.2 = ((bf16[128,3,2048]{2,1,0:T(4,128)(2,1)}), bf16[128,3,2048]{2,1,0:T(4,128)(2,1)}, u32[]{:S(2)}, u32[]{:S(2)}) async-start(bf16[128,3,2048]{2,1,0:T(4,128)(2,1)} %reshape.152), calls=%async_computation.2 | async-start | bytes 4194304 | tf_op jit(solution)/shard_map/all_to_all | solution.py:124
  392.8 8.4 %copy-start.4 = (f32[2048]{0:T(1024)S(1)}, f32[2048]{0:T(1024)}, u32[]{:S(2)}) copy-start(f32[2048]{0:T(1024)} %param.26) | copy-start | bytes 24580
Sparse Core Ops, SparseCore 0:
  9.9 73.9 all-gather.1
where the time goes:
time: 411 us; the launch traced here: 409 us
  blocking collectives  203 us (49%)
  waiting for transfers between devices  107 us (26%)
  local copies, waits for them, and re-layouts  45.1 us (11%)
  matrix products  17.9 us (4%)
  between operations  13.6 us (3%)
  other arithmetic  11.7 us (3%)
  starting transfers between devices  10.9 us (3%)
    all_to_all x1, blocking collectives, local(): lax.all_to_all(outgoing, ('sp', 'tp'), split_axis=0, concat_axis=0, tiled...  203 us
    all_gather x1, waiting for transfers between devices, local(): piece = lax.all_gather(paired, 'sp', axis=1, tiled=True)  70.6 us
    all_to_all x1, waiting for transfers between devices, local(): lax.all_to_all(expert_out.reshape(sources, slots, width_here), ('sp', 'tp...  29.7 us
  transfers between devices with their start and end apart: 3, of which 3 were waited for; matrix products, arithmetic and copies ran while one was open for 1% of the time, Pallas kernels for 0%

commit v1 on v0

--- a/solution.py
+++ b/solution.py
@@ -77,7 +77,12 @@
         )
 
     running = initial
-    piece = lax.all_gather(paired, "sp", axis=1, tiled=True)
+    ring = [paired]
+    for hop in range(15):
+        ring.append(lax.ppermute(ring[-1], "sp", [(dev, (dev + 1) % 16) for dev in range(16)]))
+    piece = jnp.roll(
+        jnp.concatenate(ring[::-1], axis=1), (lax.axis_index("sp") + 1) * ring[0].shape[1], axis=1
+    )
     row_count = piece.shape[1]
     span_rows = math.gcd(row_count, tok_dev)
 

time: 411 us -> 609 us (1.48)
  waiting for transfers between devices: 107 us -> 242 us
  local copies, waits for them, and re-layouts: 45.1 us -> 105 us
  starting transfers between devices: 10.9 us -> 27.7 us
  between operations: 13.6 us -> 0.39 us
    ppermute x0 -> x15, waiting for transfers between devices: none -> 206 us  [local(): lax.ppermute(ring[-1], 'sp', [(dev, (dev + 1) % 16) for dev in range(16)])]
    all_gather x1 -> x0, waiting for transfers between devices: 70.6 us -> none  [local(): piece = lax.all_gather(paired, 'sp', axis=1, tiled=True)]
    unnamed x21 -> x95, local copies, waits for them, and re-layouts: 4.41 us -> 56.6 us
    all_to_all x1, starting transfers between devices: 5.12 us -> 19.7 us  [local(): lax.all_to_all(attended, 'tp', split_axis=0, concat_axis=1, tiled=True)]
    dynamic_slice x0 -> x1, local copies, waits for them, and re-layouts: none -> 7.54 us  [local(): jnp.roll(jnp.concatenate(ring[::-1], axis=1), (lax.axis_index('sp') + 1)...]
  transfers between devices with their start and end apart: 3 -> 17, of which waited for: 3 -> 17; matrix products, arithmetic and copies ran while one was open for 1% -> 1% of each run, Pallas kernels for 0% -> 0%
where the time goes in v1:
time: 609 us; the launch traced here: 606 us
  waiting for transfers between devices  242 us (40%)
  blocking collectives  199 us (33%)
  local copies, waits for them, and re-layouts  105 us (17%)
  starting transfers between devices  27.7 us (5%)
  matrix products  17.9 us (3%)
  other arithmetic  13.8 us (2%)
    ppermute x15, waiting for transfers between devices, local(): lax.ppermute(ring[-1], 'sp', [(dev, (dev + 1) % 16) for dev in range(16)])  206 us
    all_to_all x1, blocking collectives, local(): lax.all_to_all(outgoing, ('sp', 'tp'), split_axis=0, concat_axis=0, tiled...  199 us
    unnamed x95, local copies, waits for them, and re-layouts  56.6 us
    all_to_all x1, waiting for transfers between devices, local(): lax.all_to_all(expert_out.reshape(sources, slots, width_here), ('sp', 'tp...  29.7 us
    all_to_all x1, starting transfers between devices, local(): lax.all_to_all(attended, 'tp', split_axis=0, concat_axis=1, tiled=True)  19.7 us
  transfers between devices with their start and end apart: 17, of which 17 were waited for; matrix products, arithmetic and copies ran while one was open for 1% of the time, Pallas kernels for 0%

profile of v1, /device:TPU:1, one launch (start us, length us, event | category | flops | bytes accessed | tf_op | source)
XLA Modules:
  0.0 606.2 jit_solution(13365848513844439057)
XLA Ops:
  0.0 1.2 copy.42
  1.2 1.1 copy.43
  2.4 2.1 collective-permute-start
  4.5 16.4 %collective-permute-done = bf16[2,1024,128]{1,2,0:T(8,128)(2,1)S(1)} collective-permute-done((bf16[2,1024,128]{1,2,0:T(8,128)(2,1)S(1)}, bf16[2,1024,128]{1,2,0:T(8,128)(2,1)S(1)}, u32[]{:S(2)}, u32[]{:S(2)}) %collective-permute-start) | collective-permute-done | bytes 524320 | tf_op jit(solution)/shard_map/ppermute | solution.py:82
  20.9 15.5 %collective-permute-done.1 = bf16[2,1024,128]{1,2,0:T(8,128)(2,1)S(1)} collective-permute-done((bf16[2,1024,128]{1,2,0:T(8,128)(2,1)S(1)}, bf16[2,1024,128]{1,2,0:T(8,128)(2,1)S(1)}, u32[]{:S(2)}, u32[]{:S(2)}) %collective-permute-start.1) | collective-permute-done | bytes 524320 | tf_op jit(solution)/shard_map/ppermute | solution.py:82
  37.2 14.7 %collective-permute-done.2 = bf16[2,1024,128]{1,2,0:T(8,128)(2,1)S(1)} collective-permute-done((bf16[2,1024,128]{1,2,0:T(8,128)(2,1)S(1)}, bf16[2,1024,128]{1,2,0:T(8,128)(2,1)S(1)}, u32[]{:S(2)}, u32[]{:S(2)}) %collective-permute-start.2) | collective-permute-done | bytes 524320 | tf_op jit(solution)/shard_map/ppermute | solution.py:82
  52.7 13.8 %collective-permute-done.3 = bf16[2,1024,128]{1,2,0:T(8,128)(2,1)S(1)} collective-permute-done((bf16[2,1024,128]{1,2,0:T(8,128)(2,1)S(1)}, bf16[2,1024,128]{1,2,0:T(8,128)(2,1)S(1)}, u32[]{:S(2)}, u32[]{:S(2)}) %collective-permute-start.3) | collective-permute-done | bytes 524320 | tf_op jit(solution)/shard_map/ppermute | solution.py:82
  67.4 13.0 %collective-permute-done.4 = bf16[2,1024,128]{1,2,0:T(8,128)(2,1)S(1)} collective-permute-done((bf16[2,1024,128]{1,2,0:T(8,128)(2,1)S(1)}, bf16[2,1024,128]{1,2,0:T(8,128)(2,1)S(1)}, u32[]{:S(2)}, u32[]{:S(2)}) %collective-permute-start.4) | collective-permute-done | bytes 524320 | tf_op jit(solution)/shard_map/ppermute | solution.py:82
  81.2 12.1 %collective-permute-done.5 = bf16[2,1024,128]{1,2,0:T(8,128)(2,1)S(1)} collective-permute-done((bf16[2,1024,128]{1,2,0:T(8,128)(2,1)S(1)}, bf16[2,1024,128]{1,2,0:T(8,128)(2,1)S(1)}, u32[]{:S(2)}, u32[]{:S(2)}) %collective-permute-start.5) | collective-permute-done | bytes 524320 | tf_op jit(solution)/shard_map/ppermute | solution.py:82
  94.1 11.3 %collective-permute-done.6 = bf16[2,1024,128]{1,2,0:T(8,128)(2,1)S(1)} collective-permute-done((bf16[2,1024,128]{1,2,0:T(8,128)(2,1)S(1)}, bf16[2,1024,128]{1,2,0:T(8,128)(2,1)S(1)}, u32[]{:S(2)}, u32[]{:S(2)}) %collective-permute-start.6) | collective-permute-done | bytes 524320 | tf_op jit(solution)/shard_map/ppermute | solution.py:82
  106.3 11.3 %collective-permute-done.7 = bf16[2,1024,128]{1,2,0:T(8,128)(2,1)S(1)} collective-permute-done((bf16[2,1024,128]{1,2,0:T(8,128)(2,1)S(1)}, bf16[2,1024,128]{1,2,0:T(8,128)(2,1)S(1)}, u32[]{:S(2)}, u32[]{:S(2)}) %collective-permute-start.7) | collective-permute-done | bytes 524320 | tf_op jit(solution)/shard_map/ppermute | solution.py:82
  118.4 11.9 %collective-permute-done.8 = bf16[2,1024,128]{1,2,0:T(8,128)(2,1)S(1)} collective-permute-done((bf16[2,1024,128]{1,2,0:T(8,128)(2,1)S(1)}, bf16[2,1024,128]{1,2,0:T(8,128)(2,1)S(1)}, u32[]{:S(2)}, u32[]{:S(2)}) %collective-permute-start.8) | collective-permute-done | bytes 524320 | tf_op jit(solution)/shard_map/ppermute | solution.py:82
  131.2 13.1 %collective-permute-done.9 = bf16[2,1024,128]{1,2,0:T(8,128)(2,1)S(1)} collective-permute-done((bf16[2,1024,128]{1,2,0:T(8,128)(2,1)S(1)}, bf16[2,1024,128]{1,2,0:T(8,128)(2,1)S(1)}, u32[]{:S(2)}, u32[]{:S(2)}) %collective-permute-start.9) | collective-permute-done | bytes 524320 | tf_op jit(solution)/shard_map/ppermute | solution.py:82
  145.1 14.2 %collective-permute-done.10 = bf16[2,1024,128]{1,2,0:T(8,128)(2,1)S(1)} collective-permute-done((bf16[2,1024,128]{1,2,0:T(8,128)(2,1)S(1)}, bf16[2,1024,128]{1,2,0:T(8,128)(2,1)S(1)}, u32[]{:S(2)}, u32[]{:S(2)}) %collective-permute-start.10) | collective-permute-done | bytes 524320 | tf_op jit(solution)/shard_map/ppermute | solution.py:82
  160.1 15.4 %collective-permute-done.11 = bf16[2,1024,128]{1,2,0:T(8,128)(2,1)S(1)} collective-permute-done((bf16[2,1024,128]{1,2,0:T(8,128)(2,1)S(1)}, bf16[2,1024,128]{1,2,0:T(8,128)(2,1)S(1)}, u32[]{:S(2)}, u32[]{:S(2)}) %collective-permute-start.11) | collective-permute-done | bytes 524320 | tf_op jit(solution)/shard_map/ppermute | solution.py:82
  176.3 16.6 %collective-permute-done.12 = bf16[2,1024,128]{1,2,0:T(8,128)(2,1)} collective-permute-done((bf16[2,1024,128]{1,2,0:T(8,128)(2,1)S(1)}, bf16[2,1024,128]{1,2,0:T(8,128)(2,1)}, u32[]{:S(2)}, u32[]{:S(2)}) %collective-permute-start.12) | collective-permute-done | bytes 524320 | tf_op jit(solution)/shard_map/ppermute | solution.py:82
  194.3 15.1 %collective-permute-done.13 = bf16[2,1024,128]{1,2,0:T(8,128)(2,1)} collective-permute-done((bf16[2,1024,128]{1,2,0:T(8,128)(2,1)}, bf16[2,1024,128]{1,2,0:T(8,128)(2,1)}, u32[]{:S(2)}, u32[]{:S(2)}) %collective-permute-start.13) | collective-permute-done | bytes 524320 | tf_op jit(solution)/shard_map/ppermute | solution.py:82
  209.5 1.8 copy.44
  212.5 1.2 broadcast_multiply_fusion
  213.8 11.1 %collective-permute-done.14 = bf16[2,1024,128]{1,2,0:T(8,128)(2,1)} collective-permute-done((bf16[2,1024,128]{1,2,0:T(8,128)(2,1)}, bf16[2,1024,128]{1,2,0:T(8,128)(2,1)}, u32[]{:S(2)}, u32[]{:S(2)}) %collective-permute-start.14) | collective-permute-done | bytes 524320 | tf_op jit(solution)/shard_map/ppermute | solution.py:82
  224.9 1.9 constant_dynamic-update-slice_fusion.31
  226.7 1.9 constant_dynamic-update-slice_fusion.30
  228.6 1.9 constant_dynamic-update-slice_fusion.29
  230.5 1.9 constant_dynamic-update-slice_fusion.28
  232.3 1.9 constant_dynamic-update-slice_fusion.27
  234.2 1.9 constant_dynamic-update-slice_fusion.26
  236.1 1.9 constant_dynamic-update-slice_fusion.25
  237.9 1.8 constant_dynamic-update-slice_fusion.24
  239.8 1.8 constant_dynamic-update-slice_fusion.23
  241.6 1.9 constant_dynamic-update-slice_fusion.22
  243.5 1.9 constant_dynamic-update-slice_fusion.21
  245.3 1.9 constant_dynamic-update-slice_fusion.20
  247.2 1.9 constant_dynamic-update-slice_fusion.19
  249.1 1.9 constant_dynamic-update-slice_fusion.18
  252.6 1.9 constant_dynamic-update-slice_fusion.15
  254.5 1.9 constant_dynamic-update-slice_fusion.14
  256.4 1.9 constant_dynamic-update-slice_fusion.13
  260.0 0.9 constant_dynamic-update-slice_fusion.10
  269.2 7.5 %constant_dynamic-slice_fusion.4 = bf16[2,16384,128]{1,2,0:T(8,128)(2,1)} fusion(bf16[2,32768,128]{1,2,0:T(8,128)(2,1)} %constant_dynamic-update-slice_fusion, s32[]{:T(128)S(6)} %select_n.55), kind=kLoop, calls=%fused_computation.101 | loop fusion | bytes 16777220 | tf_op jit(solution)/shard_map/jit(_roll_dynamic)/dynamic_slice | solution.py:83
  276.8 11.8 %while.18 = (s32[]{:T(128)}, f32[2,1024]{1,0:T(2,128)S(1)}, f32[2,1024]{1,0:T(2,128)S(1)}, f32[1024,2,64]{0,2,1:T(8,128)S(1)}, s32[]{:T(128)}, /*index=5*/s32[]{...) while((s32[]{:T(128)}, f32[2,1024]{1,0:T(2,128)S(1)}, ...), condition=%wide.region_5.6_spmd, body=%wide.region_0.5_spmd.sunk | while | flops 578035712 | bytes 32457040 | solution.py:99
  276.9 11.2 %conditional.2 = ((f32[2,1024]{1,0:T(2,128)S(1)}, f32[2,1024]{1,0:T(2,128)S(1)}, f32[1024,2,64]{0,2,1:T(8,128)S(1)})) conditional(s32[]{:T(128)} %convert_element_type.89, (f32[2,1024]{1,0:T(2,128)S(1)}, f32[2,1024]{1,0:T(2,128)S(1)}, f32[1024,2,64]{0,2,1:T(8,128)S(1)}) %tuple.52, (s32[]{:T(128)}, s32[]{:T(128)}, bf16[2,16384,128]{1,2,0:T(8,128)(2,1)}, ...), branch_computations={%region_1.1_spmd, %region_2.4_spmd} | conditional | flops 578035712 | bytes 32456802 | solution.py:92
  277.6 1.1 constant_dynamic-slice_fusion.2
  279.4 2.4 fusion.2
  281.8 3.2 fusion.9
  285.0 3.0 fusion.1
  289.5 19.7 %all-to-all-start = ((bf16[8,128,128]{1,2,0:T(8,128)(2,1)}), bf16[8,128,128]{1,2,0:T(8,128)(2,1)S(1)}, u32[]{:S(2)}, u32[]{:S(2)}) async-start(bf16[8,128,128]{1,2,0:T(8,128)(2,1)} %copy.45), calls=%async_computation | async-start | bytes 524288 | tf_op jit(solution)/shard_map/all_to_all | solution.py:104
  309.5 6.2 %all-to-all-done = bf16[8,128,128]{1,2,0:T(8,128)(2,1)S(1)} async-done(((bf16[8,128,128]{1,2,0:T(8,128)(2,1)}), bf16[8,128,128]{1,2,0:T(8,128)(2,1)S(1)}, u32[]{:S(2)}, u32[]{:S(2)}) %all-to-all-start) | async-done | bytes 262176 | tf_op jit(solution)/shard_map/all_to_all | solution.py:104
  315.7 3.0 multiply_reduce_fusion.2
  319.4 1.6 broadcast_in_dim.62
  321.0 2.3 reshape.167
  323.3 4.1 scatter_custom_fusion
  327.4 5.2 reshape.150
  332.5 199.1 %all_to_all.29 = bf16[128,3,2048]{2,1,0:T(4,128)(2,1)} all-to-all(bf16[128,3,2048]{2,1,0:T(4,128)(2,1)} %reshape.150), channel_id=1, replica_groups=mesh['sp'=16,'tp'=8] {'sp','tp'}, dimensions={0} | all-to-all | bytes 3145728 | tf_op jit(solution)/shard_map/all_to_all | solution.py:122
  531.6 5.1 reshape.151
  536.7 4.0 fusion.19
  540.7 5.3 convolution_convert_fusion
  546.0 5.2 reshape.152
  551.1 5.8 all-to-all-start.2
  557.1 29.7 %all-to-all-done.2 = bf16[128,3,2048]{2,1,0:T(4,128)(2,1)} async-done(((bf16[128,3,2048]{2,1,0:T(4,128)(2,1)}), bf16[128,3,2048]{2,1,0:T(4,128)(2,1)}, u32[]{:S(2)}, u32[]{:S(2)}) %all-to-all-start.2) | async-done | bytes 1572896 | tf_op jit(solution)/shard_map/all_to_all | solution.py:129
  586.8 5.1 reshape.153
  591.9 4.9 gather_fusion
  596.8 3.3 reshape.154
  600.2 4.8 multiply_reduce_fusion
  605.2 1.0 fusion.30
  (140 shorter events, 26.8 us)
Async XLA Ops:
  0.0 540.6 %copy-start = (bf16[1,512,2048]{2,1,0:T(8,128)(2,1)S(1)}, bf16[1,512,2048]{2,1,0:T(8,128)(2,1)}, u32[]{:S(2)}) copy-start(bf16[1,512,2048]{2,1,0:T(8,128)(2,1)} %param.31) | copy-start | bytes 6291460
  2.4 18.5 %collective-permute-start = (bf16[2,1024,128]{1,2,0:T(8,128)(2,1)S(1)}, bf16[2,1024,128]{1,2,0:T(8,128)(2,1)S(1)}, u32[]{:S(2)}, u32[]{:S(2)}) collective-permute-start(bf16[2,1024,128]{1,2,0:T(8,128)(2,1)S(1)} %pad_maximum_fusion), channel_id=1, source_target_pairs={{0,8},{8,16},{16,24},{24,32},{32,40},{40,48},{48,56},{56,64},{64,7... | collective-permute-start | bytes 1572872 | tf_op jit(solution)/shard_map/ppermute | solution.py:82
  20.9 15.6 %collective-permute-start.1 = (bf16[2,1024,128]{1,2,0:T(8,128)(2,1)S(1)}, bf16[2,1024,128]{1,2,0:T(8,128)(2,1)S(1)}, u32[]{:S(2)}, u32[]{:S(2)}) collective-permute-start(bf16[2,1024,128]{1,2,0:T(8,128)(2,1)S(1)} %collective-permute-done), channel_id=1, source_target_pairs={{0,8},{8,16},{16,24},{24,32},{32,40},{40,48},{48,56},{56,64},{64,7... | collective-permute-start | bytes 1572872 | tf_op jit(solution)/shard_map/ppermute | solution.py:82
  36.4 0.8 copy-start.1
  37.2 14.7 %collective-permute-start.2 = (bf16[2,1024,128]{1,2,0:T(8,128)(2,1)S(1)}, bf16[2,1024,128]{1,2,0:T(8,128)(2,1)S(1)}, u32[]{:S(2)}, u32[]{:S(2)}) collective-permute-start(bf16[2,1024,128]{1,2,0:T(8,128)(2,1)S(1)} %collective-permute-done.1), channel_id=1, source_target_pairs={{0,8},{8,16},{16,24},{24,32},{32,40},{40,48},{48,56},{56,64},{64,7... | collective-permute-start | bytes 1572872 | tf_op jit(solution)/shard_map/ppermute | solution.py:82
  51.9 0.8 copy-start.3
  52.7 13.8 %collective-permute-start.3 = (bf16[2,1024,128]{1,2,0:T(8,128)(2,1)S(1)}, bf16[2,1024,128]{1,2,0:T(8,128)(2,1)S(1)}, u32[]{:S(2)}, u32[]{:S(2)}) collective-permute-start(bf16[2,1024,128]{1,2,0:T(8,128)(2,1)S(1)} %collective-permute-done.2), channel_id=1, source_target_pairs={{0,8},{8,16},{16,24},{24,32},{32,40},{40,48},{48,56},{56,64},{64,7... | collective-permute-start | bytes 1572872 | tf_op jit(solution)/shard_map/ppermute | solution.py:82
  66.6 0.8 copy-start.5
  67.4 13.0 %collective-permute-start.4 = (bf16[2,1024,128]{1,2,0:T(8,128)(2,1)S(1)}, bf16[2,1024,128]{1,2,0:T(8,128)(2,1)S(1)}, u32[]{:S(2)}, u32[]{:S(2)}) collective-permute-start(bf16[2,1024,128]{1,2,0:T(8,128)(2,1)S(1)} %collective-permute-done.3), channel_id=1, source_target_pairs={{0,8},{8,16},{16,24},{24,32},{32,40},{40,48},{48,56},{56,64},{64,7... | collective-permute-start | bytes 1572872 | tf_op jit(solution)/shard_map/ppermute | solution.py:82
  80.4 0.8 copy-start.7
  81.1 12.1 %collective-permute-start.5 = (bf16[2,1024,128]{1,2,0:T(8,128)(2,1)S(1)}, bf16[2,1024,128]{1,2,0:T(8,128)(2,1)S(1)}, u32[]{:S(2)}, u32[]{:S(2)}) collective-permute-start(bf16[2,1024,128]{1,2,0:T(8,128)(2,1)S(1)} %collective-permute-done.4), channel_id=1, source_target_pairs={{0,8},{8,16},{16,24},{24,32},{32,40},{40,48},{48,56},{56,64},{64,7... | collective-permute-start | bytes 1572872 | tf_op jit(solution)/shard_map/ppermute | solution.py:82
  93.3 0.8 copy-start.9
  94.1 11.4 %collective-permute-start.6 = (bf16[2,1024,128]{1,2,0:T(8,128)(2,1)S(1)}, bf16[2,1024,128]{1,2,0:T(8,128)(2,1)S(1)}, u32[]{:S(2)}, u32[]{:S(2)}) collective-permute-start(bf16[2,1024,128]{1,2,0:T(8,128)(2,1)S(1)} %collective-permute-done.5), channel_id=1, source_target_pairs={{0,8},{8,16},{16,24},{24,32},{32,40},{40,48},{48,56},{56,64},{64,7... | collective-permute-start | bytes 1572872 | tf_op jit(solution)/shard_map/ppermute | solution.py:82
  105.4 0.8 copy-start.11
  106.3 11.4 %collective-permute-start.7 = (bf16[2,1024,128]{1,2,0:T(8,128)(2,1)S(1)}, bf16[2,1024,128]{1,2,0:T(8,128)(2,1)S(1)}, u32[]{:S(2)}, u32[]{:S(2)}) collective-permute-start(bf16[2,1024,128]{1,2,0:T(8,128)(2,1)S(1)} %collective-permute-done.6), channel_id=1, source_target_pairs={{0,8},{8,16},{16,24},{24,32},{32,40},{40,48},{48,56},{56,64},{64,7... | collective-permute-start | bytes 1572872 | tf_op jit(solution)/shard_map/ppermute | solution.py:82
  117.6 0.8 copy-start.13
  118.4 11.9 %collective-permute-start.8 = (bf16[2,1024,128]{1,2,0:T(8,128)(2,1)S(1)}, bf16[2,1024,128]{1,2,0:T(8,128)(2,1)S(1)}, u32[]{:S(2)}, u32[]{:S(2)}) collective-permute-start(bf16[2,1024,128]{1,2,0:T(8,128)(2,1)S(1)} %collective-permute-done.7), channel_id=1, source_target_pairs={{0,8},{8,16},{16,24},{24,32},{32,40},{40,48},{48,56},{56,64},{64,7... | collective-permute-start | bytes 1572872 | tf_op jit(solution)/shard_map/ppermute | solution.py:82
  130.4 0.8 copy-start.15
  131.2 13.1 %collective-permute-start.9 = (bf16[2,1024,128]{1,2,0:T(8,128)(2,1)S(1)}, bf16[2,1024,128]{1,2,0:T(8,128)(2,1)S(1)}, u32[]{:S(2)}, u32[]{:S(2)}) collective-permute-start(bf16[2,1024,128]{1,2,0:T(8,128)(2,1)S(1)} %collective-permute-done.8), channel_id=1, source_target_pairs={{0,8},{8,16},{16,24},{24,32},{32,40},{40,48},{48,56},{56,64},{64,7... | collective-permute-start | bytes 1572872 | tf_op jit(solution)/shard_map/ppermute | solution.py:82
  144.3 0.8 copy-start.17
  145.1 14.2 %collective-permute-start.10 = (bf16[2,1024,128]{1,2,0:T(8,128)(2,1)S(1)}, bf16[2,1024,128]{1,2,0:T(8,128)(2,1)S(1)}, u32[]{:S(2)}, u32[]{:S(2)}) collective-permute-start(bf16[2,1024,128]{1,2,0:T(8,128)(2,1)S(1)} %collective-permute-done.9), channel_id=1, source_target_pairs={{0,8},{8,16},{16,24},{24,32},{32,40},{40,48},{48,56},{56,64},{64,7... | collective-permute-start | bytes 1572872 | tf_op jit(solution)/shard_map/ppermute | solution.py:82
  159.3 0.8 copy-start.19
  160.1 15.4 %collective-permute-start.11 = (bf16[2,1024,128]{1,2,0:T(8,128)(2,1)S(1)}, bf16[2,1024,128]{1,2,0:T(8,128)(2,1)S(1)}, u32[]{:S(2)}, u32[]{:S(2)}) collective-permute-start(bf16[2,1024,128]{1,2,0:T(8,128)(2,1)S(1)} %collective-permute-done.10), channel_id=1, source_target_pairs={{0,8},{8,16},{16,24},{24,32},{32,40},{40,48},{48,56},{56,64},{64,7... | collective-permute-start | bytes 1572872 | tf_op jit(solution)/shard_map/ppermute | solution.py:82
  175.5 0.8 copy-start.21
  176.3 16.6 %collective-permute-start.12 = (bf16[2,1024,128]{1,2,0:T(8,128)(2,1)S(1)}, bf16[2,1024,128]{1,2,0:T(8,128)(2,1)}, u32[]{:S(2)}, u32[]{:S(2)}) collective-permute-start(bf16[2,1024,128]{1,2,0:T(8,128)(2,1)S(1)} %collective-permute-done.11), channel_id=1, source_target_pairs={{0,8},{8,16},{16,24},{24,32},{32,40},{40,48},{48,56},{56,64},{64,7... | collective-permute-start | bytes 1572872 | tf_op jit(solution)/shard_map/ppermute | solution.py:82
  193.0 16.4 %collective-permute-start.13 = (bf16[2,1024,128]{1,2,0:T(8,128)(2,1)}, bf16[2,1024,128]{1,2,0:T(8,128)(2,1)}, u32[]{:S(2)}, u32[]{:S(2)}) collective-permute-start(bf16[2,1024,128]{1,2,0:T(8,128)(2,1)} %collective-permute-done.12), channel_id=1, source_target_pairs={{0,8},{8,16},{16,24},{24,32},{32,40},{40,48},{48,56},{56,64},{64,7... | collective-permute-start | bytes 1572872 | tf_op jit(solution)/shard_map/ppermute | solution.py:82
  209.3 15.5 %collective-permute-start.14 = (bf16[2,1024,128]{1,2,0:T(8,128)(2,1)}, bf16[2,1024,128]{1,2,0:T(8,128)(2,1)}, u32[]{:S(2)}, u32[]{:S(2)}) collective-permute-start(bf16[2,1024,128]{1,2,0:T(8,128)(2,1)} %collective-permute-done.13), channel_id=1, source_target_pairs={{0,8},{8,16},{16,24},{24,32},{32,40},{40,48},{48,56},{56,64},{64,7... | collective-permute-start | bytes 1572872 | tf_op jit(solution)/shard_map/ppermute | solution.py:82
  211.4 47.0 %copy-start.22 = (bf16[2,1024,128]{1,2,0:T(8,128)(2,1)S(1)}, bf16[2,1024,128]{1,2,0:T(8,128)(2,1)}, u32[]{:S(2)}) copy-start(bf16[2,1024,128]{1,2,0:T(8,128)(2,1)} %copy-done.21) | copy-start | bytes 1572868
  211.4 47.8 %copy-start.20 = (bf16[2,1024,128]{1,2,0:T(8,128)(2,1)S(1)}, bf16[2,1024,128]{1,2,0:T(8,128)(2,1)}, u32[]{:S(2)}) copy-start(bf16[2,1024,128]{1,2,0:T(8,128)(2,1)} %copy-done.19) | copy-start | bytes 1572868
  211.4 48.6 %copy-start.18 = (bf16[2,1024,128]{1,2,0:T(8,128)(2,1)S(1)}, bf16[2,1024,128]{1,2,0:T(8,128)(2,1)}, u32[]{:S(2)}) copy-start(bf16[2,1024,128]{1,2,0:T(8,128)(2,1)} %copy-done.17) | copy-start | bytes 1572868
  211.4 49.5 %copy-start.16 = (bf16[2,1024,128]{1,2,0:T(8,128)(2,1)S(1)}, bf16[2,1024,128]{1,2,0:T(8,128)(2,1)}, u32[]{:S(2)}) copy-start(bf16[2,1024,128]{1,2,0:T(8,128)(2,1)} %copy-done.15) | copy-start | bytes 1572868
  211.4 50.3 %copy-start.14 = (bf16[2,1024,128]{1,2,0:T(8,128)(2,1)S(1)}, bf16[2,1024,128]{1,2,0:T(8,128)(2,1)}, u32[]{:S(2)}) copy-start(bf16[2,1024,128]{1,2,0:T(8,128)(2,1)} %copy-done.13) | copy-start | bytes 1572868
  211.4 51.1 %copy-start.12 = (bf16[2,1024,128]{1,2,0:T(8,128)(2,1)S(1)}, bf16[2,1024,128]{1,2,0:T(8,128)(2,1)}, u32[]{:S(2)}) copy-start(bf16[2,1024,128]{1,2,0:T(8,128)(2,1)} %copy-done.11) | copy-start | bytes 1572868
  211.4 51.9 %copy-start.10 = (bf16[2,1024,128]{1,2,0:T(8,128)(2,1)S(1)}, bf16[2,1024,128]{1,2,0:T(8,128)(2,1)}, u32[]{:S(2)}) copy-start(bf16[2,1024,128]{1,2,0:T(8,128)(2,1)} %copy-done.9) | copy-start | bytes 1572868
  211.4 52.8 %copy-start.8 = (bf16[2,1024,128]{1,2,0:T(8,128)(2,1)S(1)}, bf16[2,1024,128]{1,2,0:T(8,128)(2,1)}, u32[]{:S(2)}) copy-start(bf16[2,1024,128]{1,2,0:T(8,128)(2,1)} %copy-done.7) | copy-start | bytes 1572868
  211.5 53.6 %copy-start.6 = (bf16[2,1024,128]{1,2,0:T(8,128)(2,1)S(1)}, bf16[2,1024,128]{1,2,0:T(8,128)(2,1)}, u32[]{:S(2)}) copy-start(bf16[2,1024,128]{1,2,0:T(8,128)(2,1)} %copy-done.5) | copy-start | bytes 1572868
  211.5 54.4 %copy-start.4 = (bf16[2,1024,128]{1,2,0:T(8,128)(2,1)S(1)}, bf16[2,1024,128]{1,2,0:T(8,128)(2,1)}, u32[]{:S(2)}) copy-start(bf16[2,1024,128]{1,2,0:T(8,128)(2,1)} %copy-done.3) | copy-start | bytes 1572868
  211.5 55.2 %copy-start.2 = (bf16[2,1024,128]{1,2,0:T(8,128)(2,1)S(1)}, bf16[2,1024,128]{1,2,0:T(8,128)(2,1)}, u32[]{:S(2)}) copy-start(bf16[2,1024,128]{1,2,0:T(8,128)(2,1)} %copy-done.1) | copy-start | bytes 1572868
  254.5 22.3 %copy-start.24 = (bf16[1024,128]{0,1:T(8,128)(2,1)S(1)}, bf16[1024,128]{0,1:T(8,128)(2,1)}, u32[]{:S(2)}) copy-start(bf16[1024,128]{0,1:T(8,128)(2,1)} %copy.44) | copy-start | bytes 786436
  276.8 42.0 %copy-start.23 = (bf16[128,2048]{1,0:T(8,128)(2,1)S(1)}, bf16[128,2048]{1,0:T(8,128)(2,1)}, u32[]{:S(2)}) copy-start(bf16[128,2048]{1,0:T(8,128)(2,1)} %param.22) | copy-start | bytes 1572868
  276.8 42.0 %copy-start.25 = (f32[2048]{0:T(1024)S(1)}, f32[2048]{0:T(1024)}, u32[]{:S(2)}) copy-start(f32[2048]{0:T(1024)} %param.24) | copy-start | bytes 24580
  276.8 42.4 %copy-start.26 = (f32[2048]{0:T(1024)S(1)}, f32[2048]{0:T(1024)}, u32[]{:S(2)}) copy-start(f32[2048]{0:T(1024)} %param.25) | copy-start | bytes 24580
  289.5 26.2 %all-to-all-start = ((bf16[8,128,128]{1,2,0:T(8,128)(2,1)}), bf16[8,128,128]{1,2,0:T(8,128)(2,1)S(1)}, u32[]{:S(2)}, u32[]{:S(2)}) async-start(bf16[8,128,128]{1,2,0:T(8,128)(2,1)} %copy.45), calls=%async_computation | async-start | bytes 524288 | tf_op jit(solution)/shard_map/all_to_all | solution.py:104
  332.5 224.4 %copy-start.28 = (f32[128,2]{0,1:T(2,128)S(1)}, f32[128,2]{0,1:T(2,128)}, u32[]{:S(2)}) copy-start(f32[128,2]{0,1:T(2,128)} %param.28) | copy-start | bytes 3076
  546.0 59.2 %copy-start.27 = (f32[2048]{0:T(1024)S(1)}, f32[2048]{0:T(1024)}, u32[]{:S(2)}) copy-start(f32[2048]{0:T(1024)} %param.26) | copy-start | bytes 24580
  551.1 35.7 %all-to-all-start.2 = ((bf16[128,3,2048]{2,1,0:T(4,128)(2,1)}), bf16[128,3,2048]{2,1,0:T(4,128)(2,1)}, u32[]{:S(2)}, u32[]{:S(2)}) async-start(bf16[128,3,2048]{2,1,0:T(4,128)(2,1)} %reshape.152), calls=%async_computation.2 | async-start | bytes 4194304 | tf_op jit(solution)/shard_map/all_to_all | solution.py:129
